TPU v7x, 256 devices: a whole 4x4x8 slice. The times are simulated.
256 devices in a mesh: ep: 64 (over z, y, core), tp: 4 (over x).
Axes of the slice: x: 4, y: 4, z: 8, core: 2. Of those that a mesh axis runs over, the one named last changes fastest.
Arguments:
- queries: bfloat16 [16384, 8, 128], P('ep', 'tp'), may hold values from -15 to 15
- keys: bfloat16 [16384, 4, 128], P('ep', 'tp'), may hold values from -6 to 6
- values: bfloat16 [16384, 4, 128], P('ep', 'tp'), may hold values from -6 to 6
- key_bias: bfloat16 [16384, 8], P('ep', 'tp'), may hold values from -20 to 2
- out_weight: bfloat16 [1024, 2048], P('tp'), may hold values from -0.1875 to 0.1875
- tokens_b: bfloat16 [32768, 2048], P(('ep', 'tp')), may hold values from -6 to 6
- moe_gain: bfloat16 [2048], replicated, may hold values from 0.099609375 to 1.8984375
- gate_weight: bfloat16 [64, 2048, 2048], P('ep', None, 'tp'), may hold values from -0.125 to 0.125
- up_weight: bfloat16 [64, 2048, 2048], P('ep', None, 'tp'), may hold values from -0.125 to 0.125
- down_weight: bfloat16 [64, 2048, 2048], P('ep', 'tp'), may hold values from -0.125 to 0.125
- routes: int32 [32768, 2], P(('ep', 'tp')), may hold values from 0 to 63, all different within a row; in each aligned block of 128 rows (0 to 127, 128 to 255, ...) at most 6 rows name the same one
- route_weights: float32 [32768, 2], P(('ep', 'tp')), may hold values from 0.2 to 1
Outputs:
- mixed: bfloat16 [16384, 2048], P(('ep', 'tp'))
- moe_out: bfloat16 [32768, 2048], P(('ep', 'tp'))
Inputs may be any that keep to these rules, and one draw needn't show every extreme that they name: `routes`: each row names 2 different experts. In each aligned block of 128 rows (the rows of one device) no expert is named by more than 6 rows, and in some block one expert is named by exactly 6 rows.
All inputs are finite; a program needn't handle non-finite values.
Results may differ from a plain program's by a relative error of at most 0.012.
Values may be sent and summed in bfloat16 or wider, within the bound.
A program may use at most 128 MiB of HBM per device.

v0:
```python
import math
import jax
import jax.numpy as jnp
from jax import lax
from jax.sharding import PartitionSpec as P


def in_one_piece(arrays, axis, dim, along):
    columns = [a.reshape(*a.shape[:along], -1) for a in arrays]
    both = jnp.concatenate(columns, axis=along)
    filled, at, done = (lax.all_gather(both, axis, axis=dim, tiled=True), 0, [])
    for a, column in zip(arrays, columns):
        share = filled[..., at : at + column.shape[along]]
        done.append(share.reshape(*share.shape[:along], *a.shape[along:]))
        at += column.shape[along]
    return tuple(done)


def partner(value, axis, apart):
    mask = 2**apart
    pairs = [(source, source ^ mask) for source in range(lax.axis_size(axis))]
    return lax.ppermute(value, axis, pairs)


def split_up(value, dim, length):
    before, after = (value.shape[:dim], value.shape[dim + 1 :])
    return jnp.moveaxis(value.reshape(*before, length, -1, *after), dim, 0)


def summed_on_arrival(value, axis, dim):
    pieces = split_up(value, dim, lax.axis_size(axis))
    arrived = lax.all_to_all(pieces, axis, split_axis=0, concat_axis=0, tiled=True)
    return arrived.astype(jnp.float32).sum(axis=0)


def entry_slots(routes, expert_total):
    flattened_expert_list = routes.reshape(-1)
    onehot = (
        flattened_expert_list[:, None] == jnp.arange(expert_total, dtype=jnp.int32)[None, :]
    ).astype(jnp.int32)
    earlier_count = jnp.cumsum(onehot, axis=0) - onehot
    return (flattened_expert_list, jnp.sum(earlier_count * onehot, axis=1))


def swiglu_rows(piece, gate_cols, up_cols):
    gate_val = jnp.dot(piece, gate_cols, preferred_element_type=jnp.float32)
    up_val = jnp.dot(piece, up_cols, preferred_element_type=jnp.float32)
    return (jax.nn.silu(gate_val) * up_val).astype(jnp.bfloat16)


def attend_rows(query_block, first_pos, keys_all, values_all, bias_all, local_kv):
    row_count, local_heads, head_dim = query_block.shape
    group_size = local_heads // local_kv
    key_total = keys_all.shape[0]
    key_span = min(1024, key_total)
    query_pos = first_pos + jnp.arange(row_count, dtype=jnp.int32)
    query_rows = query_block.reshape(row_count, local_kv, group_size, head_dim)
    visit_total = (first_pos + row_count + key_span - 1) // key_span
    score_scale = 1.0 / math.sqrt(head_dim)

    def visit(visit_no, state):
        accum, carried = state
        begin_at = (visit_total - 1 - visit_no) * key_span
        key_tile_rows = lax.dynamic_slice_in_dim(keys_all, begin_at, key_span, 0)
        value_block = lax.dynamic_slice_in_dim(values_all, begin_at, key_span, 0)
        bias_block = (
            lax.dynamic_slice_in_dim(bias_all, begin_at, key_span, 0)
            .astype(jnp.float32)
            .reshape(key_span, local_kv, group_size)
        )
        scores = (
            jnp.einsum(
                "rkgd,skd->kgrs", query_rows, key_tile_rows, preferred_element_type=jnp.float32
            )
            * score_scale
        )
        scores = scores + jnp.transpose(bias_block, (1, 2, 0))[:, :, None, :]
        key_pos = begin_at + jnp.arange(key_span, dtype=jnp.int32)
        earlier = key_pos[None, :] < query_pos[:, None]
        log_keep = jnp.where(earlier, jax.nn.log_sigmoid(-scores), 0.0)
        after = lax.cumsum(log_keep, axis=3, reverse=True) - log_keep
        weights = jnp.where(
            earlier, jnp.exp(jax.nn.log_sigmoid(scores) + after + carried[..., None]), 0.0
        ).astype(jnp.bfloat16)
        accum = accum + jnp.einsum(
            "kgrs,skd->kgrd", weights, value_block, preferred_element_type=jnp.float32
        )
        return (accum, carried + jnp.sum(log_keep, axis=3))

    start_state = (
        jnp.zeros((local_kv, group_size, row_count, head_dim), jnp.float32),
        jnp.zeros((local_kv, group_size, row_count), jnp.float32),
    )
    accum = lax.fori_loop(0, visit_total, visit, start_state)[0]
    return (
        jnp.transpose(accum, (2, 0, 1, 3))
        .reshape(row_count, local_heads * head_dim)
        .astype(jnp.bfloat16)
    )


def body(
    queries,
    keys,
    values,
    key_bias,
    out_weight,
    tokens_b,
    moe_gain,
    gate_weight,
    up_weight,
    down_weight,
    routes,
    route_weights,
):
    tok_rows, local_heads, head_dim = queries.shape
    local_kv = keys.shape[1]
    ep_count = lax.axis_size("ep")
    keys_all, values_all, bias_all = in_one_piece((keys, values, key_bias), "ep", 0, 1)
    device_ep = lax.axis_index("ep")
    half_rows = tok_rows // 2
    bit_count = ep_count.bit_length() - 1
    handed = queries[half_rows:]
    for bit_no in range(bit_count):
        handed = partner(handed, "ep", bit_no)
    companion_batch = ep_count - 1 - device_ep
    own_part = attend_rows(
        queries[:half_rows], device_ep * tok_rows, keys_all, values_all, bias_all, local_kv
    )
    other_part = attend_rows(
        handed, companion_batch * tok_rows + half_rows, keys_all, values_all, bias_all, local_kv
    )
    for bit_no in range(bit_count):
        other_part = partner(other_part, "ep", bit_no)
    attended = jnp.concatenate((own_part, other_part), axis=0)
    tok_b, model_width = tokens_b.shape
    top_count = routes.shape[1]
    expert_total = ep_count * gate_weight.shape[0]
    capacity = max(2, 3 * top_count * tok_b // (2 * expert_total))
    tokens_f = tokens_b.astype(jnp.float32)
    normed = (
        tokens_f
        * lax.rsqrt(jnp.mean(tokens_f * tokens_f, axis=1, keepdims=True) + 1e-06)
        * moe_gain.astype(jnp.float32)
    ).astype(jnp.bfloat16)
    flattened_expert_list, slot_index = entry_slots(routes, expert_total)
    place = flattened_expert_list * capacity + slot_index
    outbound = (
        jnp.zeros((expert_total * capacity, model_width), jnp.bfloat16)
        .at[place]
        .set(jnp.repeat(normed, top_count, axis=0))
    )
    outbound = outbound.reshape(expert_total, capacity, model_width)
    gate_cols = gate_weight[0]
    up_cols = up_weight[0]
    down_rows = down_weight[0]
    arrived = lax.all_to_all(outbound, "ep", split_axis=0, concat_axis=0, tiled=True)
    hidden = swiglu_rows(
        lax.all_gather(arrived.reshape(ep_count * capacity, model_width), "tp", axis=0, tiled=True),
        gate_cols,
        up_cols,
    )
    mixed_sum = lax.psum_scatter(
        jnp.dot(attended, out_weight, preferred_element_type=jnp.float32).astype(jnp.bfloat16),
        "tp",
        scatter_dimension=0,
        tiled=True,
    )
    expert_sum = summed_on_arrival(
        jnp.dot(hidden, down_rows, preferred_element_type=jnp.float32).astype(jnp.bfloat16), "tp", 0
    )
    returned = lax.all_to_all(
        expert_sum.astype(jnp.bfloat16).reshape(ep_count, capacity, model_width),
        "ep",
        split_axis=0,
        concat_axis=0,
        tiled=True,
    )
    picked = jnp.take(returned.reshape(expert_total * capacity, model_width), place, axis=0).astype(
        jnp.float32
    )
    weighted = picked * route_weights.reshape(-1)[:, None]
    moe_out = jnp.sum(weighted.reshape(tok_b, top_count, model_width), axis=1).astype(jnp.bfloat16)
    return (mixed_sum, moe_out)


def solution(mesh):
    in_specs = (
        P("ep", "tp", None),
        P("ep", "tp", None),
        P("ep", "tp", None),
        P("ep", "tp"),
        P("tp", None),
        P(("ep", "tp"), None),
        P(),
        P("ep", None, "tp"),
        P("ep", None, "tp"),
        P("ep", "tp", None),
        P(("ep", "tp"), None),
        P(("ep", "tp"), None),
    )
    out_specs = (P(("ep", "tp"), None), P(("ep", "tp"), None))
    return jax.shard_map(body, mesh=mesh, in_specs=in_specs, out_specs=out_specs, check_vma=False)
```

profile of v0, /device:TPU:8, one launch (start us, length us, event | category | flops | bytes accessed | tf_op | source)
XLA Modules:
  0.0 583.5 jit_solution(1064137814376958959)
XLA Ops:
  15.4 4.1 scatter_custom_fusion
  19.5 3.7 reshape.326
  23.2 63.4 %all_to_all.15 = bf16[64,6,2048]{2,1,0:T(8,128)(2,1)} all-to-all(bf16[64,6,2048]{2,1,0:T(8,128)(2,1)} %reshape.326), channel_id=1, replica_groups=mesh['ep'=64,'tp'=4] {'ep'}, dimensions={0} | all-to-all | bytes 3145728 | tf_op jit(solution)/shard_map/all_to_all | solution.py:157
  86.7 3.8 reshape.327
  93.4 3.7 collective-permute-done.1
  97.1 2.1 collective-permute-start.2
  99.2 3.7 collective-permute-done.2
  103.5 3.6 collective-permute-done.3
  107.3 5.1 collective-permute-done.4
  113.9 41.0 %all-gather.5.cloned.1.call-done = bf16[1536,2048]{1,0:T(8,128)(2,1)} async-done(((bf16[384,2048]{1,0:T(8,128)(2,1)}), bf16[1536,2048]{1,0:T(8,128)(2,1)}) %all-gather.5.cloned.1.call-update) | async-done | bytes 6291472 | tf_op jit(solution)/shard_map/all_gather | solution.py:159
  155.0 8.6 %fusion.53 = f32[1536,512]{1,0:T(8,128)} fusion(bf16[1536,2048]{1,0:T(8,128)(2,1)} %all-gather.5.cloned.1.call-done, bf16[1,2048,512]{2,1,0:T(8,128)(2,1)} %param.23), kind=kOutput, calls=%fused_computation.82 | convolution fusion | flops 3221225472 | bytes 11534336 | tf_op jit(solution)/shard_map/dot_general | solution.py:46
  163.6 11.8 %convolution_convert_fusion = bf16[1536,2048]{1,0:T(8,128)(2,1)} fusion(bf16[1,512,2048]{2,1,0:T(8,128)(2,1)S(1)} %copy-done, bf16[1536,2048]{1,0:T(8,128)(2,1)} %all-gather.5.cloned.1.call-done, f32[1536,512]{1,0:T(8,128)} %fusion.53, bf16[1,2048,512]{2,1,0:T(8,128)(2,1)} %param.24), kind=kOutput, calls=%fused_computation.74 | convolution fusion | flops 6450315264 | bytes 19922944 | tf_op jit(solution)/shard_map/dot_general | solution.py:170
  175.3 5.3 all-to-all-start.1
  180.6 66.6 %all-gather.3.cloned.1.call-done = bf16[16384,258]{1,0:T(8,128)(2,1)} async-done(((bf16[256,258]{1,0:T(8,128)(2,1)}), bf16[16384,258]{1,0:T(8,128)(2,1)}) %all-gather.3.cloned.1.call-update) | async-done | bytes 8454160 | tf_op jit(solution)/shard_map/all_gather | solution.py:11
  247.2 5.7 slice_bitcast_fusion.4
  252.9 3.8 slice.59
  256.7 3.7 copy.53
  260.5 125.5 %while.31 = (s32[]{:T(128)}, f32[1,2,128,128]{3,2,1,0:T(8,128)S(1)}, f32[1,2,128]{2,1,0:T(2,128)S(1)}, s32[]{:T(128)}, s32[]{:T(128)}, /*index=5*/bf16[16384,1,1...) while((s32[]{:T(128)}, ...), condition=%wide.region_9.10_spmd.clone, body=%wide.region_5.9_spmd.clone.sunk | while | flops 176343936 | bytes 10775775 | solution.py:94
  260.8 1.9 fusion.99
  262.7 2.5 fusion.100
  268.6 1.9 fusion.99
  270.5 2.5 fusion.100
  276.5 1.9 fusion.99
  278.4 2.5 fusion.100
  284.3 1.9 fusion.99
  286.2 2.5 fusion.100
  292.2 1.9 fusion.99
  294.1 2.5 fusion.100
  300.0 1.9 fusion.99
  301.9 2.5 fusion.100
  307.8 1.9 fusion.99
  309.7 2.5 fusion.100
  315.7 1.9 fusion.99
  317.6 2.5 fusion.100
  323.5 1.9 fusion.99
  325.4 2.5 fusion.100
  331.4 1.9 fusion.99
  333.3 2.5 fusion.100
  339.2 1.9 fusion.99
  341.1 2.5 fusion.100
  347.1 1.9 fusion.99
  349.0 2.5 fusion.100
  354.9 1.9 fusion.99
  356.8 2.5 fusion.100
  362.7 1.9 fusion.99
  364.6 2.5 fusion.100
  370.6 1.9 fusion.99
  372.5 2.5 fusion.100
  380.3 2.5 fusion.100
  387.5 2.0 collective-permute-start.7
  389.4 2.5 collective-permute-done.7
  391.9 5.8 collective-permute-done.8
  397.7 4.3 collective-permute-done.9
  402.0 5.3 collective-permute-done.10
  407.3 4.2 reduce_sum.69
  413.1 10.0 %all-to-all-start.2 = ((bf16[64,6,2048]{2,1,0:T(8,128)(2,1)}), bf16[64,6,2048]{2,1,0:T(8,128)(2,1)}, u32[]{:S(2)}, u32[]{:S(2)}) async-start(bf16[64,6,2048]{2,1,0:T(8,128)(2,1)} %reshape.329), calls=%async_computation.3 | async-start | bytes 4194304 | tf_op jit(solution)/shard_map/all_to_all | solution.py:172
  423.2 8.1 %while.30 = (s32[]{:T(128)}, f32[1,2,128,128]{3,2,1,0:T(8,128)S(1)}, f32[1,2,128]{2,1,0:T(2,128)S(1)}, s32[]{:T(128)}, s32[]{:T(128)}, /*index=5*/bf16[16384,1,1...) while((s32[]{:T(128)}, ...), condition=%wide.region_4.5_spmd.clone, body=%wide.region_0.4_spmd.clone.sunk | while | flops 176343936 | bytes 10775775 | solution.py:94
  425.4 2.5 fusion.93
  431.4 2.7 convolution_convert_fusion.1
  434.6 39.7 %all-to-all-done.2 = bf16[64,6,2048]{2,1,0:T(8,128)(2,1)} async-done(((bf16[64,6,2048]{2,1,0:T(8,128)(2,1)}), bf16[64,6,2048]{2,1,0:T(8,128)(2,1)}, u32[]{:S(2)}, u32[]{:S(2)}) %all-to-all-start.2) | async-done | bytes 1572896 | tf_op jit(solution)/shard_map/all_to_all | solution.py:172
  474.3 3.7 reshape.330
  478.0 4.1 gather_fusion
  483.6 6.2 %multiply_reduce_fusion = bf16[128,2048]{1,0:T(8,128)(2,1)} fusion(bf16[128,2,2048]{2,1,0:T(2,128)(2,1)} %gather.7, pred[128,2]{1,0:T(8,128)(4,1)S(1)} %copy.62, f32[128,2]{1,0:T(8,128)S(1)} %copy.64), kind=kLoop, calls=%fused_computation.84 | loop fusion | flops 1835008 | bytes 1574144 | tf_op jit(solution)/shard_map/reduce_sum | solution.py:183
  489.9 86.8 %reduce-scatter.2.cloned.1.call-done = bf16[64,2048]{1,0:T(8,128)(2,1)} async-done(((bf16[256,2048]{1,0:T(8,128)(2,1)}), bf16[64,2048]{1,0:T(8,128)(2,1)}) %reduce-scatter.2.cloned.1.call-update) | async-done | bytes 262160 | tf_op jit(solution)/shard_map/reduce_scatter | solution.py:163
  (264 shorter events, 78.7 us)
Async XLA Ops:
  7.2 156.4 %copy-start = (bf16[1,512,2048]{2,1,0:T(8,128)(2,1)S(1)}, bf16[1,512,2048]{2,1,0:T(8,128)(2,1)}, u32[]{:S(2)}) copy-start(bf16[1,512,2048]{2,1,0:T(8,128)(2,1)} %param.25) | copy-start | bytes 6291460
  7.2 147.8 %all-gather.5.cloned.1.call-start = ((), (), s32[]{:S(2)}) async-start(), calls=%async_computation.6 | async-start | bytes 7864320 | tf_op jit(solution)/shard_map/all_gather | solution.py:159
  86.6 3.8 copy-start.6
  86.7 4.0 copy-start.3
  86.7 4.0 copy-start.4
  86.7 4.7 copy-start.2
  90.4 156.8 %all-gather.3.cloned.1.call-start = ((), (), s32[]{:S(2)}) async-start(), calls=%async_computation.4 | async-start | bytes 12779520 | tf_op jit(solution)/shard_map/all_gather | solution.py:11
  91.5 1.3 collective-permute-start
  92.9 4.3 collective-permute-start.1
  97.1 5.8 collective-permute-start.2
  102.9 4.3 collective-permute-start.3
  107.2 5.2 collective-permute-start.4
  112.4 148.1 %collective-permute-start.5 = (bf16[128,2,128]{2,0,1:T(8,128)(2,1)S(1)}, bf16[128,2,128]{2,0,1:T(8,128)(2,1)S(1)}, u32[]{:S(2)}, u32[]{:S(2)}) collective-permute-start(bf16[128,2,128]{2,0,1:T(8,128)(2,1)S(1)} %collective-permute-done.4), channel_id=1, source_target_pairs={{0,128},{4,132},{8,136},{12,140},{16,144},{20,148},{24,152},{28,15... | collective-permute-start | bytes 196616 | tf_op jit(solution)/shard_map/ppermute | solution.py:22
  175.3 232.0 %all-to-all-start.1 = ((bf16[4,384,2048]{2,1,0:T(8,128)(2,1)}), bf16[4,384,2048]{2,1,0:T(8,128)(2,1)}, u32[]{:S(2)}, u32[]{:S(2)}) async-start(bf16[4,384,2048]{2,1,0:T(8,128)(2,1)} %bitcast.212), calls=%async_computation.2 | async-start | bytes 12582912 | tf_op jit(solution)/shard_map/all_to_all | solution.py:32
  386.1 1.3 collective-permute-start.6
  387.5 4.5 collective-permute-start.7
  391.9 5.8 collective-permute-start.8
  397.7 4.3 collective-permute-start.9
  402.0 5.3 collective-permute-start.10
  407.3 24.1 %collective-permute-start.11 = (bf16[128,256]{0,1:T(8,128)(2,1)S(1)}, bf16[128,256]{0,1:T(8,128)(2,1)S(1)}, u32[]{:S(2)}, u32[]{:S(2)}) collective-permute-start(bf16[128,256]{0,1:T(8,128)(2,1)S(1)} %collective-permute-done.10), channel_id=1, source_target_pairs={{0,128},{4,132},{8,136},{12,140},{16,144},{20,148},{24,152},{28,15... | collective-permute-start | bytes 196616 | tf_op jit(solution)/shard_map/ppermute | solution.py:22
  413.1 61.2 %all-to-all-start.2 = ((bf16[64,6,2048]{2,1,0:T(8,128)(2,1)}), bf16[64,6,2048]{2,1,0:T(8,128)(2,1)}, u32[]{:S(2)}, u32[]{:S(2)}) async-start(bf16[64,6,2048]{2,1,0:T(8,128)(2,1)} %reshape.329), calls=%async_computation.3 | async-start | bytes 4194304 | tf_op jit(solution)/shard_map/all_to_all | solution.py:172
  423.1 153.6 %reduce-scatter.2.cloned.1.call-start = ((), (), s32[]{:S(2)}) async-start(), calls=%async_computation.5 | async-start | bytes 1310720 | tf_op jit(solution)/shard_map/reduce_scatter | solution.py:163
  431.3 3.0 copy-start.5
  431.3 3.2 copy-start.7
  478.0 98.7 %copy-start.1 = (bf16[1,512,2048]{2,1,0:T(8,128)(2,1)S(1)}, bf16[1,512,2048]{2,1,0:T(8,128)(2,1)}, u32[]{:S(2)}) copy-start(bf16[1,512,2048]{2,1,0:T(8,128)(2,1)} %param.25) | copy-start | bytes 6291460
Sparse Core Ops, SparseCore 0:
  90.6 64.3 all-gather.4
  158.3 88.9 all-gather.2
  434.2 142.4 reduce-scatter.1
where the time goes:
time: 592 us; the launch traced here: 583 us
  waiting for transfers between devices  270 us (46%)
  other arithmetic  89.5 us (15%)
  matrix products  77.4 us (13%)
  blocking collectives  63.4 us (11%)
  local copies, waits for them, and re-layouts  43.9 us (7%)
  starting transfers between devices  22.8 us (4%)
  between operations  14.2 us (2%)
    reduce_scatter x1, waiting for transfers between devices, body(): lax.psum_scatter(jnp.dot(attended, out_weight, preferred_element_type=jnp...  86.8 us
    all_gather x1, waiting for transfers between devices, in_one_piece(): filled, at, done = (lax.all_gather(both, axis, axis=dim, tiled=True), 0, [])  66.6 us
    all_to_all x1, blocking collectives, body(): lax.all_to_all(outbound, 'ep', split_axis=0, concat_axis=0, tiled=True)  63.4 us
    another operation x36, other arithmetic  44.3 us
    all_gather x1, waiting for transfers between devices, body(): lax.all_gather(arrived.reshape(ep_count * capacity, model_width), 'tp', a...  41 us
    all_to_all x1, waiting for transfers between devices, body(): lax.all_to_all(expert_sum.astype(jnp.bfloat16).reshape(ep_count, capacity...  39.7 us
    ppermute x12, waiting for transfers between devices, partner(): return lax.ppermute(value, axis, pairs)  36.2 us
    dot_general x17, matrix products, visit(): jnp.einsum('rkgd,skd->kgrs', query_rows, key_tile_rows, preferred_element...  32.2 us
  transfers between devices with their start and end apart: 17, of which 14 were waited for; matrix products, arithmetic and copies ran while one was open for 33% of the time, Pallas kernels for 0%

commit v1 on v0

--- a/solution.py
+++ b/solution.py
@@ -3,6 +3,11 @@
 import jax.numpy as jnp
 from jax import lax
 from jax.sharding import PartitionSpec as P
+
+
+def gather_from_all(x, axis, dim):
+    copies = jnp.concatenate([x] * lax.axis_size(axis), axis=dim)
+    return lax.all_to_all(copies, axis, dim, dim, tiled=True)
 
 
 def in_one_piece(arrays, axis, dim, along):
@@ -156,7 +161,7 @@
     down_rows = down_weight[0]
     arrived = lax.all_to_all(outbound, "ep", split_axis=0, concat_axis=0, tiled=True)
     hidden = swiglu_rows(
-        lax.all_gather(arrived.reshape(ep_count * capacity, model_width), "tp", axis=0, tiled=True),
+        gather_from_all(arrived.reshape(ep_count * capacity, model_width), "tp", 0),
         gate_cols,
         up_cols,
     )

time: 592 us -> 554 us (0.936)
  waiting for transfers between devices: 270 us -> 209 us
  blocking collectives: 63.4 us -> 76 us
  other arithmetic: 89.5 us -> 96.5 us
    all_gather x1, waiting for transfers between devices: 66.6 us -> 0.02 us  [in_one_piece(): filled, at, done = (lax.all_gather(both, axis, axis=dim, tiled=True), 0, [])]
    all_to_all x0 -> x1, waiting for transfers between devices: none -> 49.2 us  [gather_from_all(): return lax.all_to_all(copies, axis, dim, dim, tiled=True)]
    all_gather x1 -> x0, waiting for transfers between devices: 41 us -> none  [body(): lax.all_gather(arrived.reshape(ep_count * capacity, model_width), 'tp', a...]
    all_to_all x1, waiting for transfers between devices: 39.7 us -> 0.01 us  [body(): lax.all_to_all(expert_sum.astype(jnp.bfloat16).reshape(ep_count, capacity...]
    ppermute x12, waiting for transfers between devices: 36.2 us -> 75.2 us  [partner(): return lax.ppermute(value, axis, pairs)]
    all_to_all x1, blocking collectives: 63.4 us -> 76 us  [body(): lax.all_to_all(outbound, 'ep', split_axis=0, concat_axis=0, tiled=True)]
    concatenate x0 -> x1, other arithmetic: none -> 6.15 us  [gather_from_all(): copies = jnp.concatenate([x] * lax.axis_size(axis), axis=dim)]
  transfers between devices with their start and end apart: 17 -> 17, of which waited for: 14 -> 12; matrix products, arithmetic and copies ran while one was open for 33% -> 40% of each run, Pallas kernels for 0% -> 0%
where the time goes in v1:
time: 554 us; the launch traced here: 545 us
  waiting for transfers between devices  209 us (38%)
  other arithmetic  96.5 us (17%)
  matrix products  77.3 us (14%)
  blocking collectives  76 us (14%)
  local copies, waits for them, and re-layouts  44.6 us (8%)
  starting transfers between devices  24.9 us (4%)
  between operations  14.6 us (3%)
    reduce_scatter x1, waiting for transfers between devices, body(): lax.psum_scatter(jnp.dot(attended, out_weight, preferred_element_type=jnp...  84.5 us
    all_to_all x1, blocking collectives, body(): lax.all_to_all(outbound, 'ep', split_axis=0, concat_axis=0, tiled=True)  76 us
    ppermute x12, waiting for transfers between devices, partner(): return lax.ppermute(value, axis, pairs)  75.2 us
    all_to_all x1, waiting for transfers between devices, gather_from_all(): return lax.all_to_all(copies, axis, dim, dim, tiled=True)  49.2 us
    another operation x36, other arithmetic  44.3 us
    dot_general x17, matrix products, visit(): jnp.einsum('rkgd,skd->kgrs', query_rows, key_tile_rows, preferred_element...  32.2 us
    convert_element_type x17, other arithmetic, visit(): weights = jnp.where(earlier, jnp.exp(jax.nn.log_sigmoid(scores) + after +...  26.1 us
    dot_general x17, matrix products, visit(): jnp.einsum('kgrs,skd->kgrd', weights, value_block, preferred_element_type...  22.1 us
  transfers between devices with their start and end apart: 17, of which 12 were waited for; matrix products, arithmetic and copies ran while one was open for 40% of the time, Pallas kernels for 0%

profile of v1, /device:TPU:8, one launch (start us, length us, event | category | flops | bytes accessed | tf_op | source)
XLA Modules:
  0.0 544.8 jit_solution(1459594962895497969)
XLA Ops:
  17.8 4.1 scatter_custom_fusion
  22.0 3.7 reshape.328
  25.7 76.0 %all_to_all.27 = bf16[64,6,2048]{2,1,0:T(8,128)(2,1)} all-to-all(bf16[64,6,2048]{2,1,0:T(8,128)(2,1)} %reshape.328), channel_id=1, replica_groups=mesh['ep'=64,'tp'=4] {'ep'}, dimensions={0} | all-to-all | bytes 3145728 | tf_op jit(solution)/shard_map/all_to_all | solution.py:162
  101.7 3.7 reshape.329
  105.5 6.2 %pad_maximum_fusion = bf16[1536,2048]{1,0:T(8,128)(2,1)} fusion(bf16[384,2048]{1,0:T(8,128)(2,1)} %reshape.329), kind=kLoop, calls=%fused_computation.75 | loop fusion | flops 25165824 | bytes 7864320 | tf_op jit(solution)/shard_map/concatenate | solution.py:9
  111.6 5.4 all-to-all-start.1
  118.6 4.3 collective-permute-done.1
  124.2 4.5 collective-permute-done.2
  128.7 4.3 collective-permute-done.3
  132.9 5.3 collective-permute-done.4
  138.8 49.2 %all-to-all-done.1 = bf16[4,384,2048]{2,1,0:T(8,128)(2,1)} async-done(((bf16[4,384,2048]{2,1,0:T(8,128)(2,1)}), bf16[4,384,2048]{2,1,0:T(8,128)(2,1)}, u32[]{:S(2)}, u32[]{:S(2)}) %all-to-all-start.1) | async-done | bytes 6291488 | tf_op jit(solution)/shard_map/all_to_all | solution.py:10
  188.0 8.6 %fusion.53 = f32[1536,512]{1,0:T(8,128)} fusion(bf16[1536,2048]{1,0:T(8,128)(2,1)} %bitcast.14, bf16[1,2048,512]{2,1,0:T(8,128)(2,1)} %param.23), kind=kOutput, calls=%fused_computation.83 | convolution fusion | flops 3221225472 | bytes 11534336 | tf_op jit(solution)/shard_map/dot_general | solution.py:51
  196.6 11.8 %convolution_convert_fusion = bf16[1536,2048]{1,0:T(8,128)(2,1)} fusion(bf16[1,512,2048]{2,1,0:T(8,128)(2,1)S(1)} %copy-done, bf16[1536,2048]{1,0:T(8,128)(2,1)} %bitcast.14, f32[1536,512]{1,0:T(8,128)} %fusion.53, bf16[1,2048,512]{2,1,0:T(8,128)(2,1)} %param.24), kind=kOutput, calls=%fused_computation.74 | convolution fusion | flops 6450315264 | bytes 19922944 | tf_op jit(solution)/shard_map/dot_general | solution.py:175
  208.4 5.2 all-to-all-start.2
  213.6 5.7 %slice_bitcast_fusion.4 = (bf16[16384,1,128]{2,0,1:T(8,128)(2,1)}, bf16[16384,1,128]{2,0,1:T(8,128)(2,1)}) fusion(bf16[16384,258]{1,0:T(8,128)(2,1)} %all-gather.2.cloned.1.call-done), kind=kLoop, calls=%fused_computation.76 | loop fusion | bytes 16777216 | tf_op jit(solution)/shard_map/reshape | solution.py:19
  219.3 3.8 slice.59
  223.1 3.7 copy.53
  226.9 125.5 %while.31 = (s32[]{:T(128)}, f32[1,2,128,128]{3,2,1,0:T(8,128)S(1)}, f32[1,2,128]{2,1,0:T(2,128)S(1)}, s32[]{:T(128)}, s32[]{:T(128)}, /*index=5*/bf16[16384,1,1...) while((s32[]{:T(128)}, ...), condition=%wide.region_9.10_spmd.clone, body=%wide.region_5.9_spmd.clone.sunk | while | flops 176343936 | bytes 10775775 | solution.py:99
  227.2 1.9 fusion.99
  229.1 2.5 fusion.100
  235.0 1.9 fusion.99
  236.9 2.5 fusion.100
  242.9 1.9 fusion.99
  244.8 2.5 fusion.100
  250.7 1.9 fusion.99
  252.6 2.5 fusion.100
  258.6 1.9 fusion.99
  260.5 2.5 fusion.100
  266.4 1.9 fusion.99
  268.3 2.5 fusion.100
  274.3 1.9 fusion.99
  276.1 2.5 fusion.100
  282.1 1.9 fusion.99
  284.0 2.5 fusion.100
  289.9 1.9 fusion.99
  291.8 2.5 fusion.100
  297.8 1.9 fusion.99
  299.7 2.5 fusion.100
  305.6 1.9 fusion.99
  307.5 2.5 fusion.100
  313.5 1.9 fusion.99
  315.4 2.5 fusion.100
  321.3 1.9 fusion.99
  323.2 2.5 fusion.100
  329.2 1.9 fusion.99
  331.0 2.5 fusion.100
  337.0 1.9 fusion.99
  338.9 2.5 fusion.100
  344.8 1.9 fusion.99
  346.7 2.5 fusion.100
  354.0 4.3 collective-permute-done.7
  358.3 5.8 %collective-permute-done.8 = bf16[128,256]{0,1:T(8,128)(2,1)S(1)} collective-permute-done((bf16[128,256]{0,1:T(8,128)(2,1)S(1)}, bf16[128,256]{0,1:T(8,128)(2,1)S(1)}, u32[]{:S(2)}, u32[]{:S(2)}) %collective-permute-start.8) | collective-permute-done | bytes 65568 | tf_op jit(solution)/shard_map/ppermute | solution.py:27
  364.1 4.3 collective-permute-done.9
  368.4 4.2 reduce_sum.69
  374.1 6.4 %all-to-all-start.3 = ((bf16[64,6,2048]{2,1,0:T(8,128)(2,1)}), bf16[64,6,2048]{2,1,0:T(8,128)(2,1)}, u32[]{:S(2)}, u32[]{:S(2)}) async-start(bf16[64,6,2048]{2,1,0:T(8,128)(2,1)} %reshape.331), calls=%async_computation.4 | async-start | bytes 4194304 | tf_op jit(solution)/shard_map/all_to_all | solution.py:177
  380.6 5.6 %collective-permute-start.11 = (bf16[128,256]{0,1:T(8,128)(2,1)S(1)}, bf16[128,256]{0,1:T(8,128)(2,1)S(1)}, u32[]{:S(2)}, u32[]{:S(2)}) collective-permute-start(bf16[128,256]{0,1:T(8,128)(2,1)S(1)} %collective-permute-done.10), channel_id=1, source_target_pairs={{0,128},{4,132},{8,136},{12,140},{16,144},{20,148},{24,152},{28,15... | collective-permute-start | bytes 196616 | tf_op jit(solution)/shard_map/ppermute | solution.py:27
  386.2 8.1 %while.30 = (s32[]{:T(128)}, f32[1,2,128,128]{3,2,1,0:T(8,128)S(1)}, f32[1,2,128]{2,1,0:T(2,128)S(1)}, s32[]{:T(128)}, s32[]{:T(128)}, /*index=5*/bf16[16384,1,1...) while((s32[]{:T(128)}, ...), condition=%wide.region_4.5_spmd.clone, body=%wide.region_0.4_spmd.clone.sunk | while | flops 176343936 | bytes 10775775 | solution.py:99
  388.4 2.5 fusion.93
  394.4 40.0 %collective-permute-done.11 = bf16[128,256]{0,1:T(8,128)(2,1)S(1)} collective-permute-done((bf16[128,256]{0,1:T(8,128)(2,1)S(1)}, bf16[128,256]{0,1:T(8,128)(2,1)S(1)}, u32[]{:S(2)}, u32[]{:S(2)}) %collective-permute-start.11) | collective-permute-done | bytes 65568 | tf_op jit(solution)/shard_map/ppermute | solution.py:27
  434.4 2.7 convolution_convert_fusion.1
  437.6 3.7 reshape.332
  441.3 4.1 gather_fusion
  447.0 6.2 %multiply_reduce_fusion = bf16[128,2048]{1,0:T(8,128)(2,1)} fusion(bf16[128,2,2048]{2,1,0:T(2,128)(2,1)} %gather.7, pred[128,2]{1,0:T(8,128)(4,1)S(1)} %copy.62, f32[128,2]{1,0:T(8,128)S(1)} %copy.64), kind=kLoop, calls=%fused_computation.85 | loop fusion | flops 1835008 | bytes 1574144 | tf_op jit(solution)/shard_map/reduce_sum | solution.py:188
  453.2 84.5 %reduce-scatter.2.cloned.1.call-done = bf16[64,2048]{1,0:T(8,128)(2,1)} async-done(((bf16[256,2048]{1,0:T(8,128)(2,1)}), bf16[64,2048]{1,0:T(8,128)(2,1)}) %reduce-scatter.2.cloned.1.call-update) | async-done | bytes 262160 | tf_op jit(solution)/shard_map/reduce_scatter | solution.py:168
  (258 shorter events, 77.6 us)
Async XLA Ops:
  7.2 189.4 %copy-start = (bf16[1,512,2048]{2,1,0:T(8,128)(2,1)S(1)}, bf16[1,512,2048]{2,1,0:T(8,128)(2,1)}, u32[]{:S(2)}) copy-start(bf16[1,512,2048]{2,1,0:T(8,128)(2,1)} %param.25) | copy-start | bytes 6291460
  7.2 206.5 %all-gather.2.cloned.1.call-start = ((), (), s32[]{:S(2)}) async-start(), calls=%async_computation.5 | async-start | bytes 12779520 | tf_op jit(solution)/shard_map/all_gather | solution.py:16
  111.6 5.4 copy-start.2
  111.6 76.4 %all-to-all-start.1 = ((bf16[4,384,2048]{2,1,0:T(8,128)(2,1)}), bf16[4,384,2048]{2,1,0:T(8,128)(2,1)}, u32[]{:S(2)}, u32[]{:S(2)}) async-start(bf16[4,384,2048]{2,1,0:T(8,128)(2,1)} %bitcast.214), calls=%async_computation.2 | async-start | bytes 12582912 | tf_op jit(solution)/shard_map/all_to_all | solution.py:10
  117.2 1.4 collective-permute-start
  118.6 4.3 collective-permute-start.1
  122.9 5.8 %collective-permute-start.2 = (bf16[128,2,128]{2,0,1:T(8,128)(2,1)S(1)}, bf16[128,2,128]{2,0,1:T(8,128)(2,1)S(1)}, u32[]{:S(2)}, u32[]{:S(2)}) collective-permute-start(bf16[128,2,128]{2,0,1:T(8,128)(2,1)S(1)} %collective-permute-done.1), channel_id=1, source_target_pairs={{0,16},{4,20},{8,24},{12,28},{16,0},{20,4},{24,8},{28,12},{32,48},... | collective-permute-start | bytes 196616 | tf_op jit(solution)/shard_map/ppermute | solution.py:27
  128.7 4.3 collective-permute-start.3
  132.9 5.3 collective-permute-start.4
  138.2 88.7 %collective-permute-start.5 = (bf16[128,2,128]{2,0,1:T(8,128)(2,1)S(1)}, bf16[128,2,128]{2,0,1:T(8,128)(2,1)S(1)}, u32[]{:S(2)}, u32[]{:S(2)}) collective-permute-start(bf16[128,2,128]{2,0,1:T(8,128)(2,1)S(1)} %collective-permute-done.4), channel_id=1, source_target_pairs={{0,128},{4,132},{8,136},{12,140},{16,144},{20,148},{24,152},{28,15... | collective-permute-start | bytes 196616 | tf_op jit(solution)/shard_map/ppermute | solution.py:27
  208.4 160.0 %all-to-all-start.2 = ((bf16[4,384,2048]{2,1,0:T(8,128)(2,1)}), bf16[4,384,2048]{2,1,0:T(8,128)(2,1)}, u32[]{:S(2)}, u32[]{:S(2)}) async-start(bf16[4,384,2048]{2,1,0:T(8,128)(2,1)} %bitcast.215), calls=%async_computation.3 | async-start | bytes 12582912 | tf_op jit(solution)/shard_map/all_to_all | solution.py:37
  352.5 1.3 collective-permute-start.6
  353.9 4.4 collective-permute-start.7
  358.3 5.8 %collective-permute-start.8 = (bf16[128,256]{0,1:T(8,128)(2,1)S(1)}, bf16[128,256]{0,1:T(8,128)(2,1)S(1)}, u32[]{:S(2)}, u32[]{:S(2)}) collective-permute-start(bf16[128,256]{0,1:T(8,128)(2,1)S(1)} %collective-permute-done.7), channel_id=1, source_target_pairs={{0,16},{4,20},{8,24},{12,28},{16,0},{20,4},{24,8},{28,12},{32,48},... | collective-permute-start | bytes 196616 | tf_op jit(solution)/shard_map/ppermute | solution.py:27
  364.1 4.3 collective-permute-start.9
  368.3 12.3 %collective-permute-start.10 = (bf16[128,256]{0,1:T(8,128)(2,1)S(1)}, bf16[128,256]{0,1:T(8,128)(2,1)S(1)}, u32[]{:S(2)}, u32[]{:S(2)}) collective-permute-start(bf16[128,256]{0,1:T(8,128)(2,1)S(1)} %collective-permute-done.9), channel_id=1, source_target_pairs={{0,64},{4,68},{8,72},{12,76},{16,80},{20,84},{24,88},{28,92},{32,9... | collective-permute-start | bytes 196616 | tf_op jit(solution)/shard_map/ppermute | solution.py:27
  374.1 63.5 %all-to-all-start.3 = ((bf16[64,6,2048]{2,1,0:T(8,128)(2,1)}), bf16[64,6,2048]{2,1,0:T(8,128)(2,1)}, u32[]{:S(2)}, u32[]{:S(2)}) async-start(bf16[64,6,2048]{2,1,0:T(8,128)(2,1)} %reshape.331), calls=%async_computation.4 | async-start | bytes 4194304 | tf_op jit(solution)/shard_map/all_to_all | solution.py:177
  380.5 157.2 %reduce-scatter.2.cloned.1.call-start = ((), (), s32[]{:S(2)}) async-start(), calls=%async_computation.6 | async-start | bytes 1310720 | tf_op jit(solution)/shard_map/reduce_scatter | solution.py:168
  380.6 53.8 %collective-permute-start.11 = (bf16[128,256]{0,1:T(8,128)(2,1)S(1)}, bf16[128,256]{0,1:T(8,128)(2,1)S(1)}, u32[]{:S(2)}, u32[]{:S(2)}) collective-permute-start(bf16[128,256]{0,1:T(8,128)(2,1)S(1)} %collective-permute-done.10), channel_id=1, source_target_pairs={{0,128},{4,132},{8,136},{12,140},{16,144},{20,148},{24,152},{28,15... | collective-permute-start | bytes 196616 | tf_op jit(solution)/shard_map/ppermute | solution.py:27
  394.3 43.0 %copy-start.3 = (s32[128,2]{0,1:T(2,128)S(1)}, s32[128,2]{0,1:T(2,128)}, u32[]{:S(2)}) copy-start(s32[128,2]{0,1:T(2,128)} %param.26) | copy-start | bytes 3076
  394.3 43.2 %copy-start.4 = (f32[128,2]{0,1:T(2,128)S(1)}, f32[128,2]{0,1:T(2,128)}, u32[]{:S(2)}) copy-start(f32[128,2]{0,1:T(2,128)} %param.27) | copy-start | bytes 3076
  441.3 96.4 %copy-start.1 = (bf16[1,512,2048]{2,1,0:T(8,128)(2,1)S(1)}, bf16[1,512,2048]{2,1,0:T(8,128)(2,1)}, u32[]{:S(2)}) copy-start(bf16[1,512,2048]{2,1,0:T(8,128)(2,1)} %param.25) | copy-start | bytes 6291460
Sparse Core Ops, SparseCore 0:
  11.3 110.2 all-gather.1
  437.2 100.4 reduce-scatter.1
